TPU v7x, 32 devices: a whole 2x2x4 slice. The times are simulated.
32 devices in a mesh: grp: 2 (over y), dp: 2 (over x), kv: 4 (over z), tp: 2 (over core).
Axes of the slice: x: 2, y: 2, z: 4, core: 2. Of those that a mesh axis runs over, the one named last changes fastest.
Arguments:
- tokens: bfloat16 [32, 2048], P(('grp', 'dp'), ('kv', 'tp')), parts along dimension 0, may hold values from -40 to 40
- past_state: float32 [32, 16, 128, 128], P(('grp', 'dp', 'kv'), 'tp'), parts along dimension 0, may hold values from -4 to 4
- mix_gain: float32 [2048], P('kv'), may hold values from 0.1 to 1.9
- w_query: bfloat16 [2048, 2048], P('kv', 'tp'), may hold values from -0.125 to 0.125
- w_forget: bfloat16 [2048, 2048], P('kv', 'tp'), may hold values from -0.125 to 0.125
- w_value: bfloat16 [2048, 2048], P('kv', 'tp'), may hold values from -0.125 to 0.125
- w_gate_out: bfloat16 [2048, 2048], P('kv', 'tp'), may hold values from -0.125 to 0.125
- floor_logits: float32 [2048], P('tp'), may hold values from -6 to 6
- head_gain: float32 [128], replicated, may hold values from 0.1 to 1.9
- w_out: bfloat16 [2048, 2048], P(None, ('kv', 'tp')), may hold values from -0.125 to 0.125
- mlp_gain: float32 [2048], replicated, may hold values from 0.1 to 1.9
- w_gate: bfloat16 [2048, 5632], P(None, ('kv', 'tp')), may hold values from -0.125 to 0.125
- w_up: bfloat16 [2048, 5632], P(None, ('kv', 'tp')), may hold values from -0.125 to 0.125
- w_down: bfloat16 [5632, 2048], P(('kv', 'tp')), may hold values from -0.109375 to 0.109375
Outputs:
- result: bfloat16 [32, 2048], P(('grp', 'dp'), ('kv', 'tp')), parts along dimension 0
- new_state: float32 [32, 16, 128, 128], P(('grp', 'dp', 'kv'), 'tp'), parts along dimension 0
There are 2 independent parts, one for each index of `grp`. A program takes and returns all parts, laid end to end along the dimension named above; an argument that names none is the same for every part. Nothing has to cross between parts.
All inputs are finite; a program needn't handle non-finite values.
Results may differ from a plain program's by a relative error of at most 0.0091.
Values may be sent and summed in bfloat16 or wider, within the bound.
A program may use at most 64 MiB of HBM per device.

v0:
```python
import jax
import jax.numpy as jnp
from jax import lax
from jax.sharding import PartitionSpec as P

D = 2048
DK = 128
DV = 128


epsilon = 1e-06


def body(
    tokens,
    past_state,
    mix_gain,
    w_query,
    w_forget,
    w_value,
    w_gate_out,
    floor_logits,
    head_gain,
    w_out,
    mlp_gain,
    w_gate,
    w_up,
    w_down,
):
    kv_count = lax.axis_size("kv")
    tp_count = lax.axis_size("tp")
    rows_local = past_state.shape[0]
    heads_local = past_state.shape[1]
    width_cols = tokens.shape[1]
    own_block = lax.all_gather(tokens, "tp", axis=1, tiled=True)
    block_f = own_block.astype(jnp.float32)
    square_rows = lax.psum(jnp.sum(block_f * block_f, axis=1), "kv")
    gained = (own_block.astype(jnp.float32) * mix_gain).astype(jnp.bfloat16)
    mine = lax.dynamic_slice_in_dim(square_rows, lax.axis_index("kv") * rows_local, rows_local, 0)
    row_scale = lax.rsqrt(mine / D + epsilon)[:, None]
    query_sum, forget_sum, value_sum, gate_sum = (
        lax.psum_scatter(
            jnp.dot(gained, w_query, preferred_element_type=jnp.float32),
            "kv",
            scatter_dimension=0,
            tiled=True,
        ),
        lax.psum_scatter(
            jnp.dot(gained, w_forget, preferred_element_type=jnp.float32),
            "kv",
            scatter_dimension=0,
            tiled=True,
        ),
        lax.psum_scatter(
            jnp.dot(gained, w_value, preferred_element_type=jnp.float32),
            "kv",
            scatter_dimension=0,
            tiled=True,
        ),
        lax.psum_scatter(
            jnp.dot(gained, w_gate_out, preferred_element_type=jnp.float32),
            "kv",
            scatter_dimension=0,
            tiled=True,
        ),
    )
    query = query_sum * row_scale
    forget_pre = forget_sum * row_scale
    value = value_sum * row_scale
    gate_pre = gate_sum * row_scale
    lower = jax.nn.sigmoid(floor_logits).reshape(heads_local, DK)
    forget = lower + (1.0 - lower) * jax.nn.sigmoid(forget_pre.reshape(rows_local, heads_local, DK))
    values = value.reshape(rows_local, heads_local, DV)
    new_state = forget[..., None] * past_state + (1.0 - forget)[..., None] * values[:, :, None, :]
    activ = jax.nn.silu(query.reshape(rows_local, heads_local, DK))
    head_out = jnp.einsum("shkv,shk->shv", new_state, activ, precision=lax.Precision.HIGHEST)
    normed = head_out * lax.rsqrt(jnp.mean(head_out * head_out, axis=2, keepdims=True) + epsilon)
    normed = normed * head_gain * jax.nn.silu(gate_pre.reshape(rows_local, heads_local, DV))
    mixed = normed.reshape(1, rows_local, heads_local * DV).astype(jnp.bfloat16)
    every_head = lax.all_gather(mixed, ("kv", "tp"), axis=0, tiled=True)
    every_head = every_head.reshape(kv_count, tp_count, rows_local, heads_local * DV)
    out_blocks = w_out.reshape(tp_count, heads_local * DV, width_cols)
    projected = jnp.einsum(
        "ktsh,thc->ksc", every_head, out_blocks, preferred_element_type=jnp.float32
    )
    middle = (
        tokens.astype(jnp.float32) + projected.reshape(kv_count * rows_local, width_cols)
    ).astype(jnp.bfloat16)
    gathered = lax.all_gather(middle, ("kv", "tp"), axis=1, tiled=True)
    gathered_f = gathered.astype(jnp.float32)
    mlp_scale = lax.rsqrt(jnp.mean(gathered_f * gathered_f, axis=1, keepdims=True) + epsilon)
    mlp_in = (gathered_f * mlp_scale * mlp_gain).astype(jnp.bfloat16)
    gate = jnp.dot(mlp_in, w_gate, preferred_element_type=jnp.float32)
    upward = jnp.dot(mlp_in, w_up, preferred_element_type=jnp.float32)
    hidden = (jax.nn.silu(gate) * upward).astype(jnp.bfloat16)
    terms = jnp.dot(hidden, w_down, preferred_element_type=jnp.float32)
    summed = lax.psum_scatter(terms, ("kv", "tp"), scatter_dimension=1, tiled=True)
    result = (middle.astype(jnp.float32) + summed).astype(jnp.bfloat16)
    return (result, new_state)


def solution(mesh):
    placed = (
        P(("grp", "dp"), ("kv", "tp")),
        P(("grp", "dp", "kv"), "tp", None, None),
        P("kv"),
        P("kv", "tp"),
        P("kv", "tp"),
        P("kv", "tp"),
        P("kv", "tp"),
        P("tp"),
        P(),
        P(None, ("kv", "tp")),
        P(),
        P(None, ("kv", "tp")),
        P(None, ("kv", "tp")),
        P(("kv", "tp"), None),
    )
    return jax.shard_map(
        body,
        mesh=mesh,
        in_specs=placed,
        out_specs=(P(("grp", "dp"), ("kv", "tp")), P(("grp", "dp", "kv"), "tp", None, None)),
        check_vma=False,
    )
```

profile of v0, /device:TPU:0, one launch (start us, length us, event | category | flops | bytes accessed | tf_op | source)
XLA Modules:
  0.0 136.3 jit_solution(9865820180472469167)
XLA Ops:
  7.2 0.0 copy-start
  7.2 0.0 copy-start.8
  7.2 0.0 copy-start.4
  7.2 0.0 copy-start.6
  7.2 0.0 all-reduce.7.cloned.1.call-start
  7.3 2.2 %all_gather.9 = bf16[8,512]{1,0:T(8,128)(2,1)S(1)} all-gather(bf16[8,256]{1,0:T(8,128)(2,1)} %param.14), channel_id=1, replica_groups=mesh['grp'=2,'dp'=2,'kv'=4,'tp'=2] {'tp'}, dimensions={1}, use_global_device_ids=true | all-gather | bytes 12288 | tf_op jit(solution)/shard_map/all_gather | solution.py:35
  9.5 0.6 fusion.13
  10.1 2.1 %fusion.38 = f32[8,1024]{1,0:T(8,128)} fusion(bf16[512,1024]{1,0:T(8,128)(2,1)} %param.19, bf16[8,512]{1,0:T(8,128)(2,1)S(1)} %all_gather.9, f32[512]{0:T(512)} %param.16), kind=kOutput, calls=%fused_computation.55 | convolution fusion | flops 8400896 | bytes 1091584 | tf_op jit(solution)/shard_map/dot_general | solution.py:55
  12.2 2.1 %fusion.36 = f32[8,1024]{1,0:T(8,128)} fusion(bf16[512,1024]{1,0:T(8,128)(2,1)} %param.17, bf16[8,512]{1,0:T(8,128)(2,1)S(1)} %all_gather.9, f32[512]{0:T(512)} %param.16), kind=kOutput, calls=%fused_computation.54 | convolution fusion | flops 8400896 | bytes 1091584 | tf_op jit(solution)/shard_map/dot_general | solution.py:43
  14.3 2.1 %fusion.34 = f32[8,1024]{1,0:T(8,128)} fusion(bf16[512,1024]{1,0:T(8,128)(2,1)} %param.20, bf16[8,512]{1,0:T(8,128)(2,1)S(1)} %all_gather.9, f32[512]{0:T(512)} %param.16), kind=kOutput, calls=%fused_computation.53 | convolution fusion | flops 8400896 | bytes 1091584 | tf_op jit(solution)/shard_map/dot_general | solution.py:61
  16.5 0.9 fusion.40
  17.3 0.0 all-reduce.7.cloned.1.call-update
  17.4 0.0 reduce-scatter.2.cloned.1.call-start
  17.5 0.7 dynamic-slice
  18.8 36.2 %all-reduce.7.cloned.1.call-done = (f32[8,1024]{1,0:T(8,128)}, f32[8]{0:T(128)}, f32[8,1024]{1,0:T(8,128)}, f32[8,1024]{1,0:T(8,128)}, f32[8,1024]{1,0:T(8,128)}) async-done(((f32[8,1024]{1,0:T(8,128)}, f32[8]{0:T(128)}, f32[8,1024]{1,0:T(8,128)}, f32[8,1024]{1,0:T(8,128)}, f32[8,1024]{1,0:T(8,128)}), (f32[8,1024]{1,0:T(8,128)}, f32[8]{0:T(128)}, f32[8,1024]{1,0:T(8,128)}, f32[8,1024]{1,0:T(8,128)}, ...) | async-done | bytes 131120
  55.1 0.8 add_rsqrt_fusion.2
  55.8 0.9 fusion.24
  56.8 1.8 %multiply_add_fusion = f32[2,8,128,128]{3,2,1,0:T(8,128)S(1)} fusion(f32[2,8,128,128]{3,2,1,0:T(8,128)} %param.15, f32[2,8,128]{2,1,0:T(8,128)S(1)} %bitcast.79, f32[2,8,128]{2,1,0:T(8,128)S(1)} %get-tuple-element.7, f32[2,8,128]{2,1,0:T(8,128)S(1)} %get-tuple-element.8), kind=kLoop, calls=%fused_computation.6 | loop fusion | flops 786432 | bytes 2121728 | tf_op jit(solution)/shard_map/add | solution.py:74
  58.6 0.0 copy-start.1
  58.6 1.0 copy-done.1
  59.6 1.0 fusion.44
  60.6 0.1 multiply_reduce_fusion
  60.7 0.1 fusion.29
  60.8 14.1 %all_gather.10 = bf16[8,2,1024]{2,1,0:T(2,128)(2,1)S(1)} all-gather(bf16[1,2,1024]{2,1,0:T(2,128)(2,1)S(1)} %convert_element_type.46), channel_id=1, replica_groups=mesh['grp'=2,'dp'=2,'kv'=4,'tp'=2] {'kv','tp'}, dimensions={0}, use_global_device_ids=true | all-gather | bytes 36864 | tf_op jit(solution)/shard_map/all_gather | solution.py:80
  74.9 1.5 %fusion.3 = bf16[8,256]{1,0:T(8,128)(2,1)S(1)} fusion(bf16[8,1024,2]{1,0,2:T(8,128)(2,1)S(1)} %dot_general.37, bf16[2,1024,256]{2,1,0:T(8,128)(2,1)} %bitcast.75, bf16[8,256]{1,0:T(8,128)(2,1)S(1)} %copy-done.5), kind=kOutput, calls=%fused_computation.5 | convolution fusion | flops 8394752 | bytes 1089536 | tf_op jit(solution)/shard_map/ktsh,thc->ksc/dot_general | solution.py:83
  76.4 14.1 %all_gather.11 = bf16[8,2048]{1,0:T(8,128)(2,1)S(1)} all-gather(bf16[8,256]{1,0:T(8,128)(2,1)S(1)} %fusion.3), channel_id=1, replica_groups=mesh['grp'=2,'dp'=2,'kv'=4,'tp'=2] {'kv','tp'}, dimensions={1}, use_global_device_ids=true | all-gather | bytes 36864 | tf_op jit(solution)/shard_map/all_gather | solution.py:89
  90.5 0.1 fusion.4
  90.6 2.7 %fusion.32 = f32[8,704]{1,0:T(8,128)S(1)} fusion(bf16[2048,704]{0,1:T(8,128)(2,1)} %param.25, bf16[8,2048]{1,0:T(8,128)(2,1)S(1)} %all_gather.11, f32[2048]{0:T(1024)S(1)} %copy-done.3, f32[8]{0:T(128)S(1)} %add_rsqrt_fusion.1), kind=kOutput, calls=%fused_computation.50 | convolution fusion | flops 23134208 | bytes 2947104 | tf_op jit(solution)/shard_map/dot_general | solution.py:93
  93.3 4.1 %fusion.1 = f32[8,2048]{1,0:T(8,128)} fusion(bf16[704,2048]{1,0:T(8,128)(2,1)S(1)} %copy-done, bf16[2048,704]{0,1:T(8,128)(2,1)} %param.26, f32[8,704]{1,0:T(8,128)S(1)} %fusion.32, bf16[8,2048]{1,0:T(8,128)(2,1)S(1)} %all_gather.11, f32[2048]{0:T(1024)S(1)} %copy-done.3, f32[8]{0:T(128)S(1)} %add_rsqrt_fusion.1), kind=kOutput, calls=%fused_computation.2 | convolution fusion | flops 46236672 | bytes 5896224 | tf_op jit(solution)/shard_map/dot_general | solution.py:96
  97.4 0.0 reduce-scatter.2.cloned.1.call-update
  97.4 30.7 %reduce-scatter.2.cloned.1.call-done = f32[8,256]{1,0:T(8,128)} async-done(((f32[8,2048]{1,0:T(8,128)}), f32[8,256]{1,0:T(8,128)}) %reduce-scatter.2.cloned.1.call-update) | async-done | bytes 8208 | tf_op jit(solution)/shard_map/reduce_scatter | solution.py:97
  128.2 1.3 add_convert_fusion
  (21 shorter events, 0.1 us)
Async XLA Ops:
  7.2 86.1 %copy-start = (bf16[704,2048]{1,0:T(8,128)(2,1)S(1)}, bf16[704,2048]{1,0:T(8,128)(2,1)}, u32[]{:S(2)}) copy-start(bf16[704,2048]{1,0:T(8,128)(2,1)} %param.27) | copy-start | bytes 8650756
  7.2 10.3 %copy-start.8 = (u32[32]{0:T(128)S(1)}, u32[32]{0:T(128)}, u32[]{:S(2)}) copy-start(u32[32]{0:T(128)} %constant.38) | copy-start | bytes 388
  7.2 9.3 %copy-start.4 = (f32[512]{0:T(512)S(1)}, f32[512]{0:T(512)}, u32[]{:S(2)}) copy-start(f32[512]{0:T(512)} %param.16) | copy-start | bytes 6148
  7.2 10.2 %copy-start.6 = (f32[1024]{0:T(1024)S(1)}, f32[1024]{0:T(1024)}, u32[]{:S(2)}) copy-start(f32[1024]{0:T(1024)} %param.21) | copy-start | bytes 12292
  7.2 47.9 %all-reduce.7.cloned.1.call-start = ((), (), s32[]{:S(2)}) async-start(), calls=%async_computation.2 | async-start | bytes 263168
  7.3 9.2 %copy-start.2 = (bf16[512,1024]{1,0:T(8,128)(2,1)S(1)}, bf16[512,1024]{1,0:T(8,128)(2,1)}, u32[]{:S(2)}) copy-start(bf16[512,1024]{1,0:T(8,128)(2,1)} %param.18) | copy-start | bytes 3145732
  14.3 46.4 %copy-start.7 = (f32[128]{0:T(128)S(1)}, f32[128]{0:T(128)}, u32[]{:S(2)}) copy-start(f32[128]{0:T(128)} %param.22) | copy-start | bytes 1540
  14.3 60.6 %copy-start.5 = (bf16[8,256]{1,0:T(8,128)(2,1)S(1)}, bf16[8,256]{1,0:T(8,128)(2,1)}, u32[]{:S(2)}) copy-start(bf16[8,256]{1,0:T(8,128)(2,1)} %param.14) | copy-start | bytes 12292
  16.5 74.2 %copy-start.3 = (f32[2048]{0:T(1024)S(1)}, f32[2048]{0:T(1024)}, u32[]{:S(2)}) copy-start(f32[2048]{0:T(1024)} %param.24) | copy-start | bytes 24580
  17.4 110.8 %reduce-scatter.2.cloned.1.call-start = ((), (), s32[]{:S(2)}) async-start(), calls=%async_computation.1 | async-start | bytes 73728 | tf_op jit(solution)/shard_map/reduce_scatter | solution.py:97
  58.6 1.0 copy-start.1
Sparse Core Ops, SparseCore 0:
  17.5 37.5 all-reduce.6
  97.6 30.5 reduce-scatter.1
where the time goes:
time: 137 us; the launch traced here: 136 us
  waiting for transfers between devices  67 us (49%)
  blocking collectives  30.4 us (22%)
  matrix products  16.4 us (12%)
  between operations  14.9 us (11%)
  other arithmetic  5.75 us (4%)
  local copies, waits for them, and re-layouts  1.73 us (1%)
    unnamed x3, waiting for transfers between devices  36.3 us
    reduce_scatter x1, waiting for transfers between devices, body(): lax.psum_scatter(terms, ('kv', 'tp'), scatter_dimension=1, tiled=True)  30.7 us
    all_gather x1, blocking collectives, body(): every_head = lax.all_gather(mixed, ('kv', 'tp'), axis=0, tiled=True)  14.1 us
    all_gather x1, blocking collectives, body(): gathered = lax.all_gather(middle, ('kv', 'tp'), axis=1, tiled=True)  14.1 us
    dot_general x1, matrix products, body(): terms = jnp.dot(hidden, w_down, preferred_element_type=jnp.float32)  4.12 us
  transfers between devices with their start and end apart: 2, of which 2 were waited for; matrix products, arithmetic and copies ran while one was open for 0% of the time, Pallas kernels for 0%

commit v1 on v0

v1 whole, which is shorter than its diff:
```python
import functools

import jax
import jax.numpy as jnp
from jax import lax
from jax.experimental import pallas as pl
from jax.experimental.pallas import tpu as pltpu
from jax.sharding import PartitionSpec as P

epsilon = 1e-06
F32 = jnp.float32
BF16 = jnp.bfloat16
MESH = pl.DeviceIdType.MESH


def sigmoid(a):
    return 1.0 / (1.0 + jnp.exp(-a))


def silu(a):
    return a / (1.0 + jnp.exp(-a))


def dot_t(a, b):
    return lax.dot_general(a, b, (((1,), (1,)), ((), ())), preferred_element_type=F32)


def kernel(
    K,
    T,
    tokens,
    past,
    mix_gain,
    w_query,
    w_forget,
    w_value,
    w_gate_out,
    floor_logits,
    head_gain,
    w_out,
    mlp_gain,
    w_gate,
    w_up,
    w_down,
    result,
    new_state,
    tok_v,
    past_v,
    mixg_v,
    proj_v,
    floor_v,
    hgain_v,
    wout_v,
    mlpg_v,
    wgate_v,
    wup_v,
    wdown_v,
    new_v,
    sq_send,
    sq_recv,
    part,
    part_send,
    part_recv,
    head_v,
    mix_all,
    mix_f,
    mid_all,
    term_send,
    term_recv,
    res_v,
    local_sem,
    tok_ss,
    tok_rs,
    sq_ss,
    sq_rs,
    part_ss,
    part_rs,
    mix_ss,
    mix_rs,
    mid_ss,
    mid_rs,
    term_ss,
    term_rs,
):
    R, W = tokens.shape
    RL, H, DK, DV = past.shape
    D = w_gate.shape[1]
    kv = lax.axis_index("kv")
    tp = lax.axis_index("tp")
    me = kv * T + tp

    def far(k):
        return min(k, K - k)

    hops = sorted(range(1, K), key=far)
    near = [(0, dt) for dt in range(1, T)] + [(dk, dt) for dk in hops for dt in range(T)]

    def other(dk, dt):
        return lax.rem(kv + dk, K), lax.rem(tp + dt, T)

    def source(dk, dt):
        return lax.rem(kv + K - dk, K), lax.rem(tp + T - dt, T)

    def load(i, src, dst):
        copy = pltpu.make_async_copy(src, dst, local_sem.at[i])
        copy.start()
        return copy

    c_tok = load(0, tokens, tok_v.at[tp])
    c_mixg = load(1, mix_gain, mixg_v)
    c_proj = [
        load(2 + i, w, proj_v.at[i])
        for i, w in enumerate((w_forget, w_query, w_value, w_gate_out))
    ]
    c_past = load(6, past, past_v)
    c_floor = load(7, floor_logits, floor_v)
    c_hgain = load(8, head_gain, hgain_v)
    c_mlpg = load(9, mlp_gain, mlpg_v)
    c_wout = load(10, w_out, wout_v)
    c_wgate = load(11, w_gate, wgate_v)
    c_wup = load(12, w_up, wup_v)
    c_wdown = load(13, w_down, wdown_v)

    barrier = pltpu.get_barrier_semaphore()
    for dk, dt in near:
        k, t = other(dk, dt)
        pl.semaphore_signal(barrier, inc=1, device_id={"kv": k, "tp": t}, device_id_type=MESH)
    c_tok.wait()
    pl.semaphore_wait(barrier, len(near))

    def send(src, dst, ss, rs, k, t):
        copy = pltpu.make_async_remote_copy(
            src_ref=src,
            dst_ref=dst,
            send_sem=ss,
            recv_sem=rs,
            device_id={"kv": k, "tp": t},
            device_id_type=MESH,
        )
        copy.start()
        return copy

    def arrived(dst, ss, rs):
        pltpu.make_async_remote_copy(
            src_ref=dst,
            dst_ref=dst,
            send_sem=ss,
            recv_sem=rs,
            device_id={"kv": kv, "tp": lax.rem(tp + 1, T)},
            device_id_type=MESH,
        ).wait_recv()

    sent = []
    for dt in range(1, T):
        k, t = other(0, dt)
        sent.append(send(tok_v.at[tp], tok_v.at[tp], tok_ss.at[dt], tok_rs.at[tp], k, t))

    c_mixg.wait()
    gained = []
    square = jnp.zeros((R, 1), F32)
    for dt in range(T):
        t = lax.rem(tp + T - dt, T)
        if dt:
            arrived(tok_v.at[t], tok_ss.at[0], tok_rs.at[t])
        block = tok_v[t].astype(F32)
        square = square + jnp.sum(block * block, axis=1, keepdims=True)
        gained.append((block * mixg_v[t]).astype(BF16))
    square = jnp.broadcast_to(square, (R, DK))
    for h in range(H):
        sq_send[:, h, :] = square
    for dk in hops[::-1]:
        k, t = other(dk, 0)
        sent.append(
            send(sq_send.at[pl.ds(k * RL, RL)], sq_recv.at[kv], sq_ss.at[dk], sq_rs.at[kv], k, t)
        )
    for i in range(4):
        c_proj[i].wait()
        total = None
        for dt in range(T):
            t = lax.rem(tp + T - dt, T)
            rows = pl.ds(pl.multiple_of(t * W, W), W)
            piece = jnp.dot(gained[dt], proj_v[i, rows, :], preferred_element_type=F32)
            total = piece if total is None else total + piece
        for h in range(H):
            part[i, :, h, :] = total[:, h * DK : (h + 1) * DK]
        for k in range(K):
            part_send[i, k] = part[i, k * RL : (k + 1) * RL].reshape(RL * H, DK).astype(BF16)
        for dk in hops[::-1]:
            k, t = other(dk, 0)
            sent.append(
                send(
                    part_send.at[i, k],
                    part_recv.at[i, kv],
                    part_ss.at[i, dk],
                    part_rs.at[i, kv],
                    k,
                    t,
                )
            )

    c_floor.wait()
    c_hgain.wait()
    square = sq_send[pl.ds(kv * RL, RL)].reshape(RL * H, DK)
    for dk in hops:
        k, t = source(dk, 0)
        arrived(sq_recv.at[k], sq_ss.at[dk], sq_rs.at[k])
        square = square + sq_recv[k].reshape(RL * H, DK)
    row_scale = lax.rsqrt(square / D + epsilon)

    def summed(i):
        total = part[i, pl.ds(kv * RL, RL)].reshape(RL * H, DK)
        for dk in hops:
            k, t = source(dk, 0)
            arrived(part_recv.at[i, k], part_ss.at[i, dk], part_rs.at[i, k])
            total = total + part_recv[i, k].astype(F32)
        return total * row_scale

    lower = sigmoid(floor_v[...])
    lower = jnp.concatenate([lower] * RL, axis=0)
    forget = lower + (1.0 - lower) * sigmoid(summed(0))
    activ = silu(summed(1))
    columns = jnp.concatenate([forget, activ], axis=0).T
    value = summed(2)
    c_past.wait()
    for s in range(RL):
        for h in range(H):
            i = s * H + h
            row = value[i : i + 1, :]
            f_col = columns[:, i : i + 1]
            q_col = columns[:, RL * H + i : RL * H + i + 1]
            new = row + f_col * (past_v[s, h] - row)
            new_v[s, h] = new
            head_v[i : i + 1, :] = jnp.sum(new * q_col, axis=0, keepdims=True)
    head_out = head_v[...]
    normed = head_out * lax.rsqrt(
        jnp.mean(head_out * head_out, axis=1, keepdims=True) + epsilon
    )
    mixed = normed * hgain_v[...] * silu(summed(3))
    mix_all[tp, kv] = mixed.astype(BF16)
    for dk, dt in near[::-1]:
        k, t = other(dk, dt)
        slot = mix_all.at[tp, kv]
        sent.append(send(slot, slot, mix_ss.at[dk, dt], mix_rs.at[kv, tp], k, t))
    c_new = pltpu.make_async_copy(new_v, new_state, local_sem.at[14])
    c_new.start()

    def spread(t, k):
        mix_f[t, pl.ds(k * RL, RL)] = mix_all[t, k].astype(F32).reshape(RL, H, DV)

    spread(tp, kv)
    for dk, dt in near:
        k, t = source(dk, dt)
        arrived(mix_all.at[t, k], mix_ss.at[dk, dt], mix_rs.at[k, t])
        spread(t, k)
    every_head = jnp.concatenate(
        [mix_f[t, :, h, :].astype(BF16) for t in range(T) for h in range(H)], axis=1
    )
    c_wout.wait()
    middle = tok_v[tp].astype(F32) + jnp.dot(
        every_head, wout_v[...], preferred_element_type=F32
    )
    middle = middle.astype(BF16)
    mid_all[me] = middle
    for dk, dt in near[::-1]:
        k, t = other(dk, dt)
        slot = mid_all.at[me]
        sent.append(send(slot, slot, mid_ss.at[dk, dt], mid_rs.at[kv, tp], k, t))

    c_mlpg.wait()
    square = jnp.zeros((R, 1), F32)
    gate = None
    if W % 128 == 0:
        groups = [[peer] for peer in [(0, 0)] + near]
    else:
        groups = [[(dk, dt) for dt in range(T)] for dk in [0] + hops]
    for group in groups:
        for dk, dt in group:
            k, t = source(dk, dt)
            if dk or dt:
                arrived(mid_all.at[k * T + t], mid_ss.at[dk, dt], mid_rs.at[k, t])
        k, t = source(*group[0])
        j = k * T + (t if len(group) == 1 else 0)
        blocks = []
        for i in range(len(group)):
            block = mid_all[j + i].astype(F32)
            square = square + jnp.sum(block * block, axis=1, keepdims=True)
            blocks.append((block * mlpg_v[j + i]).astype(BF16))
        block = jnp.concatenate(blocks, axis=1) if len(blocks) > 1 else blocks[0]
        width = len(group) * W
        lanes = pl.ds(pl.multiple_of(j * W, width), width)
        if gate is None:
            c_wgate.wait()
        g = dot_t(block, wgate_v[:, lanes])
        if gate is None:
            c_wup.wait()
        u = dot_t(block, wup_v[:, lanes])
        gate, upward = (g, u) if gate is None else (gate + g, upward + u)
    mlp_scale = lax.rsqrt(square / D + epsilon)
    hidden = (silu(gate * mlp_scale) * (upward * mlp_scale)).astype(BF16)
    c_wdown.wait()
    for dk in hops[::-1] + [0]:
        k, _ = other(dk, 0)
        lanes = pl.ds(pl.multiple_of(k * T * W, T * W), T * W)
        chunk = jnp.dot(hidden, wdown_v[:, lanes], preferred_element_type=F32).astype(BF16)
        for t in range(T):
            term_send[k * T + t] = chunk[:, t * W : (t + 1) * W]
        for dt in range(0 if dk else 1, T):
            _, t = other(dk, dt)
            sent.append(
                send(
                    term_send.at[k * T + t],
                    term_recv.at[me],
                    term_ss.at[dk, dt],
                    term_rs.at[kv, tp],
                    k,
                    t,
                )
            )
    total = term_send[me].astype(F32)
    for dk, dt in near:
        k, t = source(dk, dt)
        j = k * T + t
        arrived(term_recv.at[j], term_ss.at[dk, dt], term_rs.at[k, t])
        total = total + term_recv[j].astype(F32)
    res_v[...] = (middle.astype(F32) + total).astype(BF16)
    c_res = pltpu.make_async_copy(res_v, result, local_sem.at[15])
    c_res.start()
    for copy in sent:
        copy.wait_send()
    c_new.wait()
    c_res.wait()


def body(
    tokens,
    past_state,
    mix_gain,
    w_query,
    w_forget,
    w_value,
    w_gate_out,
    floor_logits,
    head_gain,
    w_out,
    mlp_gain,
    w_gate,
    w_up,
    w_down,
):
    K = lax.axis_size("kv")
    T = lax.axis_size("tp")
    n = K * T
    R, W = tokens.shape
    RL, H, DK, DV = past_state.shape
    args = (
        tokens,
        past_state,
        mix_gain.reshape(T, 1, W),
        w_query,
        w_forget,
        w_value,
        w_gate_out,
        floor_logits.reshape(H, DK),
        head_gain.reshape(1, DV),
        w_out,
        mlp_gain.reshape(n, 1, W),
        w_gate.T,
        w_up.T,
        w_down,
    )
    V = pltpu.VMEM
    dma = pltpu.SemaphoreType.DMA
    anywhere = pl.BlockSpec(memory_space=pl.ANY)
    return pl.pallas_call(
        functools.partial(kernel, K, T),
        out_shape=(
            jax.ShapeDtypeStruct((R, W), BF16),
            jax.ShapeDtypeStruct(past_state.shape, F32),
        ),
        in_specs=[anywhere] * len(args),
        out_specs=(anywhere, anywhere),
        scratch_shapes=[
            V((T, R, W), BF16),
            V(past_state.shape, F32),
            V((T, 1, W), F32),
            V((4,) + w_query.shape, BF16),
            V((H, DK), F32),
            V((1, DV), F32),
            V(w_out.shape, BF16),
            V((n, 1, W), F32),
            V(w_gate.shape[::-1], BF16),
            V(w_up.shape[::-1], BF16),
            V(w_down.shape, BF16),
            V(past_state.shape, F32),
            V((R, H, DK), F32),
            V((K, RL, H, DK), F32),
            V((4, R, H, DK), F32),
            V((4, K, RL * H, DK), BF16),
            V((4, K, RL * H, DK), BF16),
            V((RL * H, DV), F32),
            V((T, K, RL * H, DV), BF16),
            V((T, R, H, DV), F32),
            V((n, R, W), BF16),
            V((n, R, W), BF16),
            V((n, R, W), BF16),
            V((R, W), BF16),
            dma((16,)),
            dma((T,)),
            dma((T,)),
            dma((K,)),
            dma((K,)),
            dma((4, K)),
            dma((4, K)),
            dma((K, T)),
            dma((K, T)),
            dma((K, T)),
            dma((K, T)),
            dma((K, T)),
            dma((K, T)),
        ],
        compiler_params=pltpu.CompilerParams(
            collective_id=0, has_side_effects=True, vmem_limit_bytes=60 * 1024 * 1024
        ),
    )(*args)


def solution(mesh):
    placed = (
        P(("grp", "dp"), ("kv", "tp")),
        P(("grp", "dp", "kv"), "tp", None, None),
        P("kv"),
        P("kv", "tp"),
        P("kv", "tp"),
        P("kv", "tp"),
        P("kv", "tp"),
        P("tp"),
        P(),
        P(None, ("kv", "tp")),
        P(),
        P(None, ("kv", "tp")),
        P(None, ("kv", "tp")),
        P(("kv", "tp"), None),
    )
    return jax.shard_map(
        body,
        mesh=mesh,
        in_specs=placed,
        out_specs=(P(("grp", "dp"), ("kv", "tp")), P(("grp", "dp", "kv"), "tp", None, None)),
        check_vma=False,
    )
```

time: 137 us -> 30.1 us (0.22)
  waiting for transfers between devices: 67 us -> 0 us
  blocking collectives: 30.4 us -> 0 us
  Pallas kernels: 0 us -> 25.7 us
  matrix products: 16.4 us -> 0 us
  between operations: 14.9 us -> 0.64 us
  other arithmetic: 5.75 us -> 0 us
  local copies, waits for them, and re-layouts: 1.73 us -> 3.57 us
    unnamed x3 -> x0, waiting for transfers between devices: 36.3 us -> none
    reduce_scatter x1 -> x0, waiting for transfers between devices: 30.7 us -> none  [body(): lax.psum_scatter(terms, ('kv', 'tp'), scatter_dimension=1, tiled=True)]
    all_gather x3 -> x0, blocking collectives: 30.4 us -> none  [the longest x1 14.1 us: body(): every_head = lax.all_gather(mixed, ('kv', 'tp'), axis=0, tiled=True)]
    pallas_call x0 -> x1, Pallas kernels: none -> 25.7 us  [body(): pl.pallas_call(functools.partial(kernel, K, T), out_shape=(jax.ShapeDtype...]
    dot_general x8 -> x0, matrix products: 16.4 us -> none  [the longest x1 4.12 us: body(): terms = jnp.dot(hidden, w_down, preferred_element_type=jnp.float32)]
    unnamed x20 -> x2, local copies, waits for them, and re-layouts: 1.67 us -> 3.57 us
    add x2 -> x0, other arithmetic: 1.84 us -> none  [the longest x1 1.84 us: body(): forget[..., None] * past_state]
  transfers between devices with their start and end apart: 2 -> 0, of which waited for: 2 -> 0; matrix products, arithmetic and copies ran while one was open for 0% -> 0% of each run, Pallas kernels for 0% -> 0%
where the time goes in v1:
time: 30.1 us; the launch traced here: 29.9 us
  Pallas kernels  25.7 us (85%)
  local copies, waits for them, and re-layouts  3.57 us (12%)
  between operations  0.64 us (2%)
    pallas_call x1, Pallas kernels, body(): pl.pallas_call(functools.partial(kernel, K, T), out_shape=(jax.ShapeDtype...  25.7 us
    unnamed x2, local copies, waits for them, and re-layouts  3.57 us

profile of v1, /device:TPU:0, one launch (start us, length us, event | category | flops | bytes accessed | tf_op | source)
XLA Modules:
  0.0 29.9 jit_solution(16111363224682748667)
XLA Ops:
  0.6 25.7 %shard_map.149 = (bf16[8,256]{1,0:T(8,128)(2,1)}, f32[2,8,128,128]{3,2,1,0:T(8,128)}) custom-call(bf16[8,256]{1,0:T(8,128)(2,1)} %tokens.1, f32[2,8,128,128]{3,2,1,0:T(8,128)} %past.1, f32[2,1,256]{2,1,0:T(1,128)} %bitcast.10, bf16[512,1024]{1,0:T(8,128)(2,1)} %w_query.1, bf16[512,1024]{1,0:T(8,128)(2,1)} %w_forget.1, bf16[512,1024]{1,0:T(8,128)(2,1)} %w_value.1, ...), custom_call_target="tpu_custom_call" | custom-call | tf_op jit(solution)/shard_map/pallas_call | solution.py:374
  26.3 1.3 %copy.18 = bf16[8,256]{1,0:T(8,128)(2,1)} copy(bf16[8,256]{1,0:T(8,128)(2,1)} %get-tuple-element.4) | data formatting | bytes 8192
  27.6 2.3 %copy.19 = f32[2,8,128,128]{3,2,1,0:T(8,128)} copy(f32[2,8,128,128]{3,2,1,0:T(8,128)} %get-tuple-element.5) | data formatting | bytes 2097152

commit v2 on v1

--- a/solution.py
+++ b/solution.py
@@ -55,7 +55,6 @@
     wgate_v,
     wup_v,
     wdown_v,
-    new_v,
     sq_send,
     sq_recv,
     part,
@@ -67,7 +66,6 @@
     mid_all,
     term_send,
     term_recv,
-    res_v,
     local_sem,
     tok_ss,
     tok_rs,
@@ -229,7 +227,7 @@
             f_col = columns[:, i : i + 1]
             q_col = columns[:, RL * H + i : RL * H + i + 1]
             new = row + f_col * (past_v[s, h] - row)
-            new_v[s, h] = new
+            new_state[s, h] = new
             head_v[i : i + 1, :] = jnp.sum(new * q_col, axis=0, keepdims=True)
     head_out = head_v[...]
     normed = head_out * lax.rsqrt(
@@ -241,8 +239,6 @@
         k, t = other(dk, dt)
         slot = mix_all.at[tp, kv]
         sent.append(send(slot, slot, mix_ss.at[dk, dt], mix_rs.at[kv, tp], k, t))
-    c_new = pltpu.make_async_copy(new_v, new_state, local_sem.at[14])
-    c_new.start()
 
     def spread(t, k):
         mix_f[t, pl.ds(k * RL, RL)] = mix_all[t, k].astype(F32).reshape(RL, H, DV)
@@ -322,13 +318,9 @@
         j = k * T + t
         arrived(term_recv.at[j], term_ss.at[dk, dt], term_rs.at[k, t])
         total = total + term_recv[j].astype(F32)
-    res_v[...] = (middle.astype(F32) + total).astype(BF16)
-    c_res = pltpu.make_async_copy(res_v, result, local_sem.at[15])
-    c_res.start()
+    result[...] = (middle.astype(F32) + total).astype(BF16)
     for copy in sent:
         copy.wait_send()
-    c_new.wait()
-    c_res.wait()
 
 
 def body(
@@ -374,11 +366,11 @@
     return pl.pallas_call(
         functools.partial(kernel, K, T),
         out_shape=(
-            jax.ShapeDtypeStruct((R, W), BF16),
-            jax.ShapeDtypeStruct(past_state.shape, F32),
+            pltpu.VMEM((R, W), BF16),
+            pltpu.VMEM(past_state.shape, F32),
         ),
         in_specs=[anywhere] * len(args),
-        out_specs=(anywhere, anywhere),
+        out_specs=(pl.BlockSpec(memory_space=pltpu.VMEM),)*2,
         scratch_shapes=[
             V((T, R, W), BF16),
             V(past_state.shape, F32),
@@ -391,7 +383,6 @@
             V(w_gate.shape[::-1], BF16),
             V(w_up.shape[::-1], BF16),
             V(w_down.shape, BF16),
-            V(past_state.shape, F32),
             V((R, H, DK), F32),
             V((K, RL, H, DK), F32),
             V((4, R, H, DK), F32),
@@ -403,8 +394,7 @@
             V((n, R, W), BF16),
             V((n, R, W), BF16),
             V((n, R, W), BF16),
-            V((R, W), BF16),
-            dma((16,)),
+            dma((14,)),
             dma((T,)),
             dma((T,)),
             dma((K,)),

time: 30.1 us -> 27.5 us (0.914)
  local copies, waits for them, and re-layouts: 3.57 us -> 1.56 us
  Pallas kernels: 25.7 us -> 25.1 us
    unnamed x2, local copies, waits for them, and re-layouts: 3.57 us -> 1.56 us
    pallas_call x1, Pallas kernels: 25.7 us -> 25.1 us  [body(): pl.pallas_call(functools.partial(kernel, K, T), out_shape=(pltpu.VMEM((R,...]
where the time goes in v2:
time: 27.5 us; the launch traced here: 27.3 us
  Pallas kernels  25.1 us (91%)
  local copies, waits for them, and re-layouts  1.56 us (6%)
  between operations  0.64 us (2%)
    pallas_call x1, Pallas kernels, body(): pl.pallas_call(functools.partial(kernel, K, T), out_shape=(pltpu.VMEM((R,...  25.1 us
    unnamed x2, local copies, waits for them, and re-layouts  1.56 us

profile of v2, /device:TPU:0, one launch (start us, length us, event | category | flops | bytes accessed | tf_op | source)
XLA Modules:
  0.0 27.3 jit_solution(1233750437931090565)
XLA Ops:
  0.6 25.1 %shard_map.149 = (bf16[8,256]{1,0:T(8,128)(2,1)S(1)}, f32[2,8,128,128]{3,2,1,0:T(8,128)S(1)}) custom-call(bf16[8,256]{1,0:T(8,128)(2,1)} %tokens.1, f32[2,8,128,128]{3,2,1,0:T(8,128)} %past.1, f32[2,1,256]{2,1,0:T(1,128)} %bitcast.10, bf16[512,1024]{1,0:T(8,128)(2,1)} %w_query.1, bf16[512,1024]{1,0:T(8,128)(2,1)} %w_forget.1, bf16[512,1024]{1,0:T(8,128)(2,1)} %w_value.1, ...), custom_call_target="tpu_custom_call" | custom-call | tf_op jit(solution)/shard_map/pallas_call | solution.py:366
  25.8 0.6 %copy.18 = bf16[8,256]{1,0:T(8,128)(2,1)} copy(bf16[8,256]{1,0:T(8,128)(2,1)S(1)} %get-tuple-element.2) | data formatting | bytes 8192
  26.4 1.0 %copy.19 = f32[2,8,128,128]{3,2,1,0:T(8,128)} copy(f32[2,8,128,128]{3,2,1,0:T(8,128)S(1)} %get-tuple-element.3) | data formatting | bytes 2097152

commit v3 on v2

--- a/solution.py
+++ b/solution.py
@@ -155,6 +155,7 @@
 
     c_mixg.wait()
     gained = []
+    early = []
     square = jnp.zeros((R, 1), F32)
     for dt in range(T):
         t = lax.rem(tp + T - dt, T)
@@ -163,6 +164,13 @@
         block = tok_v[t].astype(F32)
         square = square + jnp.sum(block * block, axis=1, keepdims=True)
         gained.append((block * mixg_v[t]).astype(BF16))
+        if dt == 0:
+            rows = pl.ds(pl.multiple_of(t * W, W), W)
+            for i in range(4):
+                c_proj[i].wait()
+                early.append(
+                    jnp.dot(gained[0], proj_v[i, rows, :], preferred_element_type=F32)
+                )
     square = jnp.broadcast_to(square, (R, DK))
     for h in range(H):
         sq_send[:, h, :] = square
@@ -172,13 +180,12 @@
             send(sq_send.at[pl.ds(k * RL, RL)], sq_recv.at[kv], sq_ss.at[dk], sq_rs.at[kv], k, t)
         )
     for i in range(4):
-        c_proj[i].wait()
-        total = None
-        for dt in range(T):
+        total = early[i]
+        for dt in range(1, T):
             t = lax.rem(tp + T - dt, T)
             rows = pl.ds(pl.multiple_of(t * W, W), W)
             piece = jnp.dot(gained[dt], proj_v[i, rows, :], preferred_element_type=F32)
-            total = piece if total is None else total + piece
+            total = total + piece
         for h in range(H):
             part[i, :, h, :] = total[:, h * DK : (h + 1) * DK]
         for k in range(K):

time: 27.5 us -> 27.5 us (level)
  no operation moved by 1% of the time
where the time goes in v3:
time: 27.5 us; the launch traced here: 27.3 us
  Pallas kernels  25.1 us (91%)
  local copies, waits for them, and re-layouts  1.56 us (6%)
  between operations  0.64 us (2%)
    pallas_call x1, Pallas kernels, body(): pl.pallas_call(functools.partial(kernel, K, T), out_shape=(pltpu.VMEM((R,...  25.1 us
    unnamed x2, local copies, waits for them, and re-layouts  1.56 us

profile of v3, /device:TPU:0, one launch (start us, length us, event | category | flops | bytes accessed | tf_op | source)
XLA Modules:
  0.0 27.3 jit_solution(8585143105486297976)
XLA Ops:
  0.6 25.1 %shard_map.149 = (bf16[8,256]{1,0:T(8,128)(2,1)S(1)}, f32[2,8,128,128]{3,2,1,0:T(8,128)S(1)}) custom-call(bf16[8,256]{1,0:T(8,128)(2,1)} %tokens.1, f32[2,8,128,128]{3,2,1,0:T(8,128)} %past.1, f32[2,1,256]{2,1,0:T(1,128)} %bitcast.10, bf16[512,1024]{1,0:T(8,128)(2,1)} %w_query.1, bf16[512,1024]{1,0:T(8,128)(2,1)} %w_forget.1, bf16[512,1024]{1,0:T(8,128)(2,1)} %w_value.1, ...), custom_call_target="tpu_custom_call" | custom-call | tf_op jit(solution)/shard_map/pallas_call | solution.py:373
  25.8 0.6 %copy.18 = bf16[8,256]{1,0:T(8,128)(2,1)} copy(bf16[8,256]{1,0:T(8,128)(2,1)S(1)} %get-tuple-element.2) | data formatting | bytes 8192
  26.4 1.0 %copy.19 = f32[2,8,128,128]{3,2,1,0:T(8,128)} copy(f32[2,8,128,128]{3,2,1,0:T(8,128)S(1)} %get-tuple-element.3) | data formatting | bytes 2097152
